TPU v7x, 32 devices: a whole 2x2x4 slice. The times are simulated.
32 devices in a mesh: sp: 8 (over z, y), dp: 4 (over x, core).
Axes of the slice: x: 2, y: 2, z: 4, core: 2. Of those that a mesh axis runs over, the one named last changes fastest.
Arguments:
- queries: bfloat16 [4, 2048, 1280], P('dp', None, 'sp'), may hold values from -6 to 6
- keys: bfloat16 [4, 1024, 1280], P('dp', None, 'sp'), may hold values from -6 to 6
- values: bfloat16 [4, 1024, 1280], P('dp', None, 'sp'), may hold values from -48 to 48
- q_gain: float32 [64], replicated, may hold values from 0.5 to 10
- k_gain: float32 [64], replicated, may hold values from 0.5 to 10
- w_out: bfloat16 [2048, 2048], P(None, 'dp'), may hold values from -0.125 to 0.125
Outputs:
- mixed: bfloat16 [4, 1280, 2048], P('dp', 'sp')
All inputs are finite; a program needn't handle non-finite values.
Results may differ from a plain program's by a relative error of at most 0.0038.
The roundings to bfloat16 on the way count: a program that leaves them out, or rounds other values in their place, can miss the bound.
Values may be sent and summed in bfloat16 or wider, within the bound.
No kernel may reach another device: no remote copies, remote signals or barrier semaphores. Data moves between devices by JAX's collectives and lax.ppermute only.
A program may use at most 64 MiB of HBM per device.

v0:
```python
import jax
import jax.numpy as jnp
from jax import lax
from jax.sharding import PartitionSpec as P

HD = 64
QH = 32
KV = 16
GRID_W = 64


epsilon = 1e-06
rotary_base = 10000.0
block_count = 8


def swapped(block, axis, apart):
    count = lax.axis_size(axis)
    route = []
    for low in range(count):
        high = low | 1 << apart
        if high != low and high < count:
            route += [(low, high), (high, low)]
    return lax.ppermute(block, axis, route)


def rotary_tables(first_row, row_count):
    position = first_row + lax.iota(jnp.int32, row_count)
    grid_row = (position // GRID_W).astype(jnp.float32)
    grid_col = (position % GRID_W).astype(jnp.float32)
    quarter = HD // 4
    inv_freq = rotary_base ** (-(2.0 * lax.iota(jnp.float32, quarter)) / (HD // 2))
    row_angle = inv_freq[:, None] * grid_row[None, :]
    col_angle = inv_freq[:, None] * grid_col[None, :]
    cos_table = jnp.concatenate(
        [jnp.cos(row_angle), jnp.cos(row_angle), jnp.cos(col_angle), jnp.cos(col_angle)], axis=0
    )
    sin_table = jnp.concatenate(
        [jnp.sin(row_angle), jnp.sin(row_angle), jnp.sin(col_angle), jnp.sin(col_angle)], axis=0
    )
    return (cos_table, sin_table)


def normalize_turn(field, gain, cos_table, sin_table):
    head_count = field.shape[0] // HD
    values_f = field.astype(jnp.float32).reshape(head_count, HD, field.shape[1])
    normed = (
        values_f
        * lax.rsqrt(jnp.mean(values_f * values_f, axis=1, keepdims=True) + epsilon)
        * gain[None, :, None]
    )
    quarter = HD // 4
    quarters_of = normed.reshape(head_count, 4, quarter, field.shape[1])
    turned = jnp.concatenate(
        [-quarters_of[:, 1], quarters_of[:, 0], -quarters_of[:, 3], quarters_of[:, 2]], axis=1
    )
    return (normed * cos_table[None] + turned * sin_table[None]).astype(jnp.bfloat16)


def attention_heads(query_heads, key_heads, value_heads, seq_len):
    kv_local = key_heads.shape[0]
    group_local = query_heads.shape[0] // kv_local
    query_split = query_heads.reshape(kv_local, group_local, HD, seq_len)
    score_scale = HD ** (-0.5)
    block_rows = seq_len // block_count

    def one_block(block_index, result):
        row_start = block_index * block_rows
        query_block = lax.dynamic_slice_in_dim(query_split, row_start, block_rows, 3)
        scores = (
            jnp.einsum("hgdq,hdk->hgqk", query_block, key_heads, preferred_element_type=jnp.float32)
            * score_scale
        )
        row_max = jnp.max(scores, axis=-1, keepdims=True)
        weights = jnp.exp(scores - row_max)
        weights = (weights / jnp.sum(weights, axis=-1, keepdims=True)).astype(jnp.bfloat16)
        attended = jnp.einsum(
            "hgqk,hdk->hgdq", weights, value_heads, preferred_element_type=jnp.float32
        )
        return lax.dynamic_update_slice_in_dim(result, attended.astype(jnp.bfloat16), row_start, 3)

    result = jnp.zeros(query_split.shape, jnp.bfloat16)
    result = lax.fori_loop(0, block_count, one_block, result)
    return result.reshape(query_heads.shape)


def on_device(queries, keys, values, q_gain, k_gain, w_out):
    sp_count = lax.axis_size("sp")
    tok_rows = queries.shape[2]
    seq_len = tok_rows * sp_count
    cos_table, sin_table = rotary_tables(lax.axis_index("sp") * tok_rows, tok_rows)
    query_rot = normalize_turn(queries[0], q_gain, cos_table, sin_table)
    key_rot = normalize_turn(keys[0], k_gain, cos_table, sin_table)
    value_rows = values[0].reshape(KV, HD, tok_rows)
    query_heads = lax.all_to_all(query_rot, "sp", split_axis=0, concat_axis=2, tiled=True)
    share_count = max(sp_count // KV, 1)
    part_rows = tok_rows // share_count
    key_cut = (
        key_rot.reshape(KV, HD, share_count, part_rows)
        .transpose(0, 2, 1, 3)
        .reshape(KV * share_count, HD, part_rows)
    )
    value_cut = (
        value_rows.reshape(KV, HD, share_count, part_rows)
        .transpose(0, 2, 1, 3)
        .reshape(KV * share_count, HD, part_rows)
    )
    key_got, value_got = (
        lax.all_to_all(key_cut, "sp", split_axis=0, concat_axis=2, tiled=True),
        lax.all_to_all(value_cut, "sp", split_axis=0, concat_axis=2, tiled=True),
    )
    kv_local = key_got.shape[0]
    key_got = key_got.reshape(kv_local, HD, sp_count, part_rows)
    value_got = value_got.reshape(kv_local, HD, sp_count, part_rows)
    for bit_index in range(share_count.bit_length() - 1):
        key_other, value_other = swapped((key_got, value_got), "sp", bit_index)
        key_got = jnp.concatenate([key_got, key_other], axis=3)
        value_got = jnp.concatenate([value_got, value_other], axis=3)
    key_heads = key_got.reshape(kv_local, HD, seq_len)
    value_heads = value_got.reshape(kv_local, HD, seq_len)
    attended = attention_heads(query_heads, key_heads, value_heads, seq_len)
    token_heads = lax.all_to_all(attended, "sp", split_axis=2, concat_axis=0, tiled=True)
    token_rows = token_heads.reshape(QH * HD, tok_rows)
    product = lax.dot_general(
        token_rows,
        lax.all_gather(w_out, "dp", axis=1, tiled=True),
        (((0,), (0,)), ((), ())),
        preferred_element_type=jnp.float32,
    )
    mixed_rows = product.astype(jnp.bfloat16)
    return mixed_rows[None]


def solution(mesh):
    placed = (
        P("dp", None, "sp"),
        P("dp", None, "sp"),
        P("dp", None, "sp"),
        P(),
        P(),
        P(None, "dp"),
    )
    return jax.shard_map(
        on_device, mesh=mesh, in_specs=placed, out_specs=P("dp", "sp", None), check_vma=False
    )
```

profile of v0, /device:TPU:0, one launch (start us, length us, event | category | flops | bytes accessed | tf_op | source)
XLA Modules:
  0.0 176.7 jit_solution(5040789266582131515)
XLA Ops:
  7.3 1.3 reshape.101
  9.3 3.6 %copy.58 = f32[16,4,16,160]{2,0,3,1:T(8,128)} copy(f32[16,4,16,160]{3,2,1,0:T(8,128)S(1)} %bitcast.86) | data formatting | bytes 1310720 | tf_op jit(solution)/shard_map/convert_element_type | solution.py:46
  13.4 3.1 %multiply_multiply_fusion.1 = f32[16,4,16,160]{2,0,3,1:T(8,128)S(1)} fusion(f32[16,4,16,160]{2,0,3,1:T(8,128)} %copy.58, f32[4,16]{1,0:T(4,128)S(1)} %mul.184, f32[16,160]{0,1:T(8,128)S(1)} %add_rsqrt_fusion), kind=kLoop, calls=%fused_computation.21 | loop fusion | flops 327680 | bytes 1321216 | tf_op jit(solution)/shard_map/mul | solution.py:48
  16.9 1.6 fusion.42
  18.5 1.4 copy.60
  19.8 7.3 %all-to-all-start.1 = ((bf16[16,64,160]{2,1,0:T(8,128)(2,1)}), bf16[16,64,160]{2,1,0:T(8,128)(2,1)}, u32[]{:S(2)}, u32[]{:S(2)}) async-start(bf16[16,64,160]{2,1,0:T(8,128)(2,1)} %copy.60), calls=%async_computation.1 | async-start | bytes 1048576 | tf_op jit(solution)/shard_map/all_to_all | solution.py:109
  27.1 1.0 reshape.99
  28.1 1.6 copy.51
  29.7 10.7 %copy.52 = f32[32,4,16,160]{2,0,3,1:T(8,128)} copy(f32[32,4,16,160]{3,2,1,0:T(8,128)} %bitcast.81) | data formatting | bytes 2621440 | tf_op jit(solution)/shard_map/convert_element_type | solution.py:46
  40.6 1.0 copy.69
  42.3 9.7 %multiply_multiply_fusion = f32[32,4,16,160]{2,0,3,1:T(8,128)} fusion(f32[32,4,16,160]{2,0,3,1:T(8,128)} %copy.52, f32[4,16]{1,0:T(4,128)S(1)} %mul.170, f32[32,160]{0,1:T(8,128)S(1)} %add_rsqrt_fusion.1), kind=kLoop, calls=%fused_computation.20 | loop fusion | flops 655360 | bytes 2642176 | tf_op jit(solution)/shard_map/mul | solution.py:48
  52.0 6.0 %all-to-all-start.2 = ((bf16[16,64,160]{2,1,0:T(8,128)(2,1)}), bf16[16,64,160]{2,1,0:T(8,128)(2,1)S(1)}, u32[]{:S(2)}, u32[]{:S(2)}) async-start(bf16[16,64,160]{2,1,0:T(8,128)(2,1)} %bitcast.88), calls=%async_computation.2 | async-start | bytes 1048576 | tf_op jit(solution)/shard_map/all_to_all | solution.py:110
  58.0 6.1 %fusion.35 = (f32[32,16,160]{1,0,2:T(8,128)S(1)}, f32[32,16,160]{1,0,2:T(8,128)S(1)}, f32[32,16,160]{1,0,2:T(8,128)S(1)}, f32[32,16,160]{1,0,2:T(8,128)S(1)}) fusion(f32[32,4,16,160]{2,0,3,1:T(8,128)} %multiply_multiply_fusion), kind=kLoop, calls=%fused_computation.27 | loop fusion | flops 163840 | bytes 2621440 | tf_op jit(solution)/shard_map/neg | solution.py:55
  64.1 3.8 %fusion.37 = bf16[32,64,160]{1,0,2:T(8,128)(2,1)} fusion(f32[32,16,160]{1,0,2:T(8,128)S(1)} %get-tuple-element.111, f32[32,16,160]{1,0,2:T(8,128)S(1)} %get-tuple-element.112, f32[32,16,160]{1,0,2:T(8,128)S(1)} %get-tuple-element.113, f32[32,16,160]{1,0,2:T(8,128)S(1)} %get-tuple-element.110, f32[32,64,160]{1,0,2:T(8,128)S(1)} %reshape.99, ...), kind=kLoop, calls=%fused_computation.30 | loop fusion | flops 2949120 | bytes 3379456 | tf_op jit(solution)/shard_map/convert_element_type | solution.py:57
  67.9 3.0 %copy.54 = bf16[32,64,160]{2,1,0:T(8,128)(2,1)} copy(bf16[32,64,160]{1,0,2:T(8,128)(2,1)} %fusion.37) | data formatting | bytes 1310720 | tf_op jit(solution)/shard_map/convert_element_type | solution.py:57
  70.8 1.1 all-to-all-done.2
  71.9 4.9 %all-to-all-start = ((bf16[32,64,160]{2,1,0:T(8,128)(2,1)}), bf16[32,64,160]{2,1,0:T(8,128)(2,1)S(1)}, u32[]{:S(2)}, u32[]{:S(2)}) async-start(bf16[32,64,160]{2,1,0:T(8,128)(2,1)} %copy.54), calls=%async_computation | async-start | bytes 2097152 | tf_op jit(solution)/shard_map/all_to_all | solution.py:95
  76.9 1.3 copy.61
  79.6 22.2 %all-to-all-done = bf16[32,64,160]{2,1,0:T(8,128)(2,1)S(1)} async-done(((bf16[32,64,160]{2,1,0:T(8,128)(2,1)}), bf16[32,64,160]{2,1,0:T(8,128)(2,1)S(1)}, u32[]{:S(2)}, u32[]{:S(2)}) %all-to-all-start) | async-done | bytes 655392 | tf_op jit(solution)/shard_map/all_to_all | solution.py:95
  102.3 1.2 reshape.96
  103.5 33.8 %while.13 = (s32[]{:T(128)}, bf16[2,2,64,1280]{3,2,1,0:T(8,128)(2,1)S(1)}, bf16[2,2,64,1280]{3,2,1,0:T(8,128)(2,1)S(1)}, bf16[2,64,1280]{2,1,0:T(8,128)(2,1)S(1)...) while((s32[]{:T(128)}, bf16[2,2,64,1280]{3,2,1,0:T(8,128)(2,1)S(1)}, ...), condition=%wide.region_5.6_spmd, body=%wide.region_2.5_spmd.sunk | while | flops 320351360 | bytes 1497751 | solution.py:83
  103.6 1.3 fusion.65
  104.9 1.8 %fusion.66 = bf16[2,2,64,160]{3,2,1,0:T(8,128)(2,1)S(1)} fusion(f32[2,2,160]{2,1,0:T(2,128)S(1)} %fusion.65, bf16[2,64,1280]{2,1,0:T(8,128)(2,1)S(1)} %get-tuple-element.179, bf16[2,64,1280]{2,1,0:T(8,128)(2,1)S(1)} %get-tuple-element.178, bf16[2,2,64,1280]{3,2,1,0:T(8,128)(2,1)S(1)} %get-tuple-element.177, s32[]{:T(128)S(6)} %select_n.37), kind=kOutput, calls=%fused_computation.7.clone.1 | convolution fusion | flops 213034880 | bytes 872452 | tf_op jit(solution)/shard_map/while/body/eval_jaxpr/hgqk,hdk->hgdq/dot_general | solution.py:77
  107.3 1.3 fusion.65
  108.6 1.8 %fusion.66 = bf16[2,2,64,160]{3,2,1,0:T(8,128)(2,1)S(1)} fusion(f32[2,2,160]{2,1,0:T(2,128)S(1)} %fusion.65, bf16[2,64,1280]{2,1,0:T(8,128)(2,1)S(1)} %get-tuple-element.179, bf16[2,64,1280]{2,1,0:T(8,128)(2,1)S(1)} %get-tuple-element.178, bf16[2,2,64,1280]{3,2,1,0:T(8,128)(2,1)S(1)} %get-tuple-element.177, s32[]{:T(128)S(6)} %select_n.37), kind=kOutput, calls=%fused_computation.7.clone.1 | convolution fusion | flops 213034880 | bytes 872452 | tf_op jit(solution)/shard_map/while/body/eval_jaxpr/hgqk,hdk->hgdq/dot_general | solution.py:77
  110.4 1.3 dynamic_update_slice.8
  111.7 1.3 fusion.65
  113.0 1.8 %fusion.66 = bf16[2,2,64,160]{3,2,1,0:T(8,128)(2,1)S(1)} fusion(f32[2,2,160]{2,1,0:T(2,128)S(1)} %fusion.65, bf16[2,64,1280]{2,1,0:T(8,128)(2,1)S(1)} %get-tuple-element.179, bf16[2,64,1280]{2,1,0:T(8,128)(2,1)S(1)} %get-tuple-element.178, bf16[2,2,64,1280]{3,2,1,0:T(8,128)(2,1)S(1)} %get-tuple-element.177, s32[]{:T(128)S(6)} %select_n.37), kind=kOutput, calls=%fused_computation.7.clone.1 | convolution fusion | flops 213034880 | bytes 872452 | tf_op jit(solution)/shard_map/while/body/eval_jaxpr/hgqk,hdk->hgdq/dot_general | solution.py:77
  114.8 1.3 dynamic_update_slice.8
  116.1 1.3 fusion.65
  117.4 1.8 %fusion.66 = bf16[2,2,64,160]{3,2,1,0:T(8,128)(2,1)S(1)} fusion(f32[2,2,160]{2,1,0:T(2,128)S(1)} %fusion.65, bf16[2,64,1280]{2,1,0:T(8,128)(2,1)S(1)} %get-tuple-element.179, bf16[2,64,1280]{2,1,0:T(8,128)(2,1)S(1)} %get-tuple-element.178, bf16[2,2,64,1280]{3,2,1,0:T(8,128)(2,1)S(1)} %get-tuple-element.177, s32[]{:T(128)S(6)} %select_n.37), kind=kOutput, calls=%fused_computation.7.clone.1 | convolution fusion | flops 213034880 | bytes 872452 | tf_op jit(solution)/shard_map/while/body/eval_jaxpr/hgqk,hdk->hgdq/dot_general | solution.py:77
  119.2 1.3 dynamic_update_slice.8
  120.6 1.3 fusion.65
  121.9 1.8 %fusion.66 = bf16[2,2,64,160]{3,2,1,0:T(8,128)(2,1)S(1)} fusion(f32[2,2,160]{2,1,0:T(2,128)S(1)} %fusion.65, bf16[2,64,1280]{2,1,0:T(8,128)(2,1)S(1)} %get-tuple-element.179, bf16[2,64,1280]{2,1,0:T(8,128)(2,1)S(1)} %get-tuple-element.178, bf16[2,2,64,1280]{3,2,1,0:T(8,128)(2,1)S(1)} %get-tuple-element.177, s32[]{:T(128)S(6)} %select_n.37), kind=kOutput, calls=%fused_computation.7.clone.1 | convolution fusion | flops 213034880 | bytes 872452 | tf_op jit(solution)/shard_map/while/body/eval_jaxpr/hgqk,hdk->hgdq/dot_general | solution.py:77
  124.3 1.3 fusion.65
  125.6 1.8 %fusion.66 = bf16[2,2,64,160]{3,2,1,0:T(8,128)(2,1)S(1)} fusion(f32[2,2,160]{2,1,0:T(2,128)S(1)} %fusion.65, bf16[2,64,1280]{2,1,0:T(8,128)(2,1)S(1)} %get-tuple-element.179, bf16[2,64,1280]{2,1,0:T(8,128)(2,1)S(1)} %get-tuple-element.178, bf16[2,2,64,1280]{3,2,1,0:T(8,128)(2,1)S(1)} %get-tuple-element.177, s32[]{:T(128)S(6)} %select_n.37), kind=kOutput, calls=%fused_computation.7.clone.1 | convolution fusion | flops 213034880 | bytes 872452 | tf_op jit(solution)/shard_map/while/body/eval_jaxpr/hgqk,hdk->hgdq/dot_general | solution.py:77
  127.4 1.3 dynamic_update_slice.8
  128.7 1.3 fusion.65
  130.0 1.8 %fusion.66 = bf16[2,2,64,160]{3,2,1,0:T(8,128)(2,1)S(1)} fusion(f32[2,2,160]{2,1,0:T(2,128)S(1)} %fusion.65, bf16[2,64,1280]{2,1,0:T(8,128)(2,1)S(1)} %get-tuple-element.179, bf16[2,64,1280]{2,1,0:T(8,128)(2,1)S(1)} %get-tuple-element.178, bf16[2,2,64,1280]{3,2,1,0:T(8,128)(2,1)S(1)} %get-tuple-element.177, s32[]{:T(128)S(6)} %select_n.37), kind=kOutput, calls=%fused_computation.7.clone.1 | convolution fusion | flops 213034880 | bytes 872452 | tf_op jit(solution)/shard_map/while/body/eval_jaxpr/hgqk,hdk->hgdq/dot_general | solution.py:77
  131.8 1.2 dynamic_update_slice.8
  133.1 1.3 fusion.65
  134.4 1.8 %fusion.66 = bf16[2,2,64,160]{3,2,1,0:T(8,128)(2,1)S(1)} fusion(f32[2,2,160]{2,1,0:T(2,128)S(1)} %fusion.65, bf16[2,64,1280]{2,1,0:T(8,128)(2,1)S(1)} %get-tuple-element.179, bf16[2,64,1280]{2,1,0:T(8,128)(2,1)S(1)} %get-tuple-element.178, bf16[2,2,64,1280]{3,2,1,0:T(8,128)(2,1)S(1)} %get-tuple-element.177, s32[]{:T(128)S(6)} %select_n.37), kind=kOutput, calls=%fused_computation.7.clone.1 | convolution fusion | flops 213034880 | bytes 872452 | tf_op jit(solution)/shard_map/while/body/eval_jaxpr/hgqk,hdk->hgdq/dot_general | solution.py:77
  136.1 1.2 dynamic_update_slice.8
  137.3 1.7 copy.64
  139.1 0.9 reshape.105
  139.9 21.1 %all_to_all.66 = bf16[8,2,20480]{2,1,0:T(2,128)(2,1)S(1)} all-to-all(bf16[8,2,20480]{2,1,0:T(2,128)(2,1)S(1)} %reshape.105), channel_id=1, replica_groups=mesh['sp'=8,'dp'=4] {'sp'}, dimensions={0} | all-to-all | bytes 1310720 | tf_op jit(solution)/shard_map/all_to_all | solution.py:122
  161.8 2.2 %copy.71 = bf16[4,64,8,160]{3,1,0,2:T(8,128)(2,1)S(1)} copy(bf16[4,64,8,160]{1,0,3,2:T(4,128)(2,1)S(1)} %bitcast.83) | data formatting | bytes 1310720 | tf_op jit(solution)/shard_map/all_to_all | solution.py:122
  164.0 5.8 %fusion.38 = bf16[1,160,2048]{2,1,0:T(8,128)(2,1)} fusion(bf16[2048,160]{1,0:T(8,128)(2,1)S(1)} %bitcast.82, bf16[2048,2048]{1,0:T(8,128)(2,1)} %all-gather.2.cloned.1.call-done), kind=kOutput, calls=%fused_computation.33 | convolution fusion | flops 1342504960 | bytes 9699328 | tf_op jit(solution)/shard_map/dot_general | solution.py:124
  (37 shorter events, 7.1 us)
Async XLA Ops:
  6.5 2.1 %copy-start.1 = (bf16[1,1024,160]{1,2,0:T(8,128)(2,1)S(1)}, bf16[1,1024,160]{1,2,0:T(8,128)(2,1)}, u32[]{:S(2)}) copy-start(bf16[1,1024,160]{1,2,0:T(8,128)(2,1)} %param.9) | copy-start | bytes 983044
  6.5 157.5 %all-gather.2.cloned.1.call-start = ((), (), s32[]{:S(2)}) async-start(), calls=%async_computation.4 | async-start | bytes 10485760 | tf_op jit(solution)/shard_map/all_gather | solution.py:126
  9.3 3.6 %copy-start.4 = (f32[64]{0:T(128)S(1)}, f32[64]{0:T(128)}, u32[]{:S(2)}) copy-start(f32[64]{0:T(128)} %param.12) | copy-start | bytes 772
  18.5 8.7 %copy-start = (bf16[1,2048,160]{1,2,0:T(8,128)(2,1)S(1)}, bf16[1,2048,160]{1,2,0:T(8,128)(2,1)}, u32[]{:S(2)}) copy-start(bf16[1,2048,160]{1,2,0:T(8,128)(2,1)} %param.8) | copy-start | bytes 1966084
  19.8 32.2 %all-to-all-start.1 = ((bf16[16,64,160]{2,1,0:T(8,128)(2,1)}), bf16[16,64,160]{2,1,0:T(8,128)(2,1)}, u32[]{:S(2)}, u32[]{:S(2)}) async-start(bf16[16,64,160]{2,1,0:T(8,128)(2,1)} %copy.60), calls=%async_computation.1 | async-start | bytes 1048576 | tf_op jit(solution)/shard_map/all_to_all | solution.py:109
  29.7 10.7 %copy-start.3 = (f32[64]{0:T(128)S(1)}, f32[64]{0:T(128)}, u32[]{:S(2)}) copy-start(f32[64]{0:T(128)} %param.11) | copy-start | bytes 772
  29.7 10.8 %copy-start.2 = (bf16[1,1024,160]{1,2,0:T(8,128)(2,1)S(1)}, bf16[1,1024,160]{1,2,0:T(8,128)(2,1)}, u32[]{:S(2)}) copy-start(bf16[1,1024,160]{1,2,0:T(8,128)(2,1)} %param.10) | copy-start | bytes 983044
  52.0 19.9 %all-to-all-start.2 = ((bf16[16,64,160]{2,1,0:T(8,128)(2,1)}), bf16[16,64,160]{2,1,0:T(8,128)(2,1)S(1)}, u32[]{:S(2)}, u32[]{:S(2)}) async-start(bf16[16,64,160]{2,1,0:T(8,128)(2,1)} %bitcast.88), calls=%async_computation.2 | async-start | bytes 1048576 | tf_op jit(solution)/shard_map/all_to_all | solution.py:110
  71.9 29.8 %all-to-all-start = ((bf16[32,64,160]{2,1,0:T(8,128)(2,1)}), bf16[32,64,160]{2,1,0:T(8,128)(2,1)S(1)}, u32[]{:S(2)}, u32[]{:S(2)}) async-start(bf16[32,64,160]{2,1,0:T(8,128)(2,1)} %copy.54), calls=%async_computation | async-start | bytes 2097152 | tf_op jit(solution)/shard_map/all_to_all | solution.py:95
Sparse Core Ops, SparseCore 0:
  8.9 60.9 all-gather.1
where the time goes:
time: 177 us
  local copies, waits for them, and re-layouts  43 us (24%)
  matrix products  30.5 us (17%)
  other arithmetic  26 us (15%)
  waiting for transfers between devices  24 us (14%)
  blocking collectives  21.1 us (12%)
  starting transfers between devices  18.2 us (10%)
  between operations  13.6 us (8%)
    all_to_all x1, waiting for transfers between devices, on_device(): lax.all_to_all(query_rot, 'sp', split_axis=0, concat_axis=2, tiled=True)  22.2 us
    all_to_all x1, blocking collectives, on_device(): lax.all_to_all(attended, 'sp', split_axis=2, concat_axis=0, tiled=True)  21.1 us
    convert_element_type x6, local copies, waits for them, and re-layouts, normalize_turn(): values_f = field.astype(jnp.float32).reshape(head_count, HD, field.shape[1])  18.4 us
    dot_general x8, matrix products, one_block(): jnp.einsum('hgqk,hdk->hgdq', weights, value_heads, preferred_element_type...  14.3 us
    mul x2, other arithmetic, normalize_turn(): values_f * lax.rsqrt(jnp.mean(values_f * values_f, axis=1, keepdims=True)...  12.8 us
    sub x8, matrix products, one_block(): weights = jnp.exp(scores - row_max)  10.4 us
    dynamic_update_slice x8, local copies, waits for them, and re-layouts, one_block(): lax.dynamic_update_slice_in_dim(result, attended.astype(jnp.bfloat16), ro...  8.81 us
    all_to_all x1, starting transfers between devices, on_device(): lax.all_to_all(key_cut, 'sp', split_axis=0, concat_axis=2, tiled=True)  7.31 us
  transfers between devices with their start and end apart: 4, of which 2 were waited for; matrix products, arithmetic and copies ran while one was open for 52% of the time, Pallas kernels for 0%

commit v1 on v0

--- a/solution.py
+++ b/solution.py
@@ -1,13 +1,18 @@
+import functools
+
 import jax
 import jax.numpy as jnp
 from jax import lax
+from jax.experimental import pallas as pl
+from jax.experimental.pallas import tpu as pltpu
 from jax.sharding import PartitionSpec as P
 
 HD = 64
 QH = 32
 KV = 16
 GRID_W = 64
-
+GROUP = QH // KV
+PAIR = GROUP * HD
 
 epsilon = 1e-06
 rotary_base = 10000.0
@@ -84,7 +89,7 @@
     return result.reshape(query_heads.shape)
 
 
-def on_device(queries, keys, values, q_gain, k_gain, w_out):
+def plain_form(queries, keys, values, q_gain, k_gain, w_out):
     sp_count = lax.axis_size("sp")
     tok_rows = queries.shape[2]
     seq_len = tok_rows * sp_count
@@ -131,6 +136,174 @@
     return mixed_rows[None]
 
 
+def turned_head(rows, gain, cos_table, sin_table):
+    field = rows.astype(jnp.float32)
+    normed = field * lax.rsqrt(jnp.mean(field * field, axis=0, keepdims=True) + epsilon) * gain
+    quarter = HD // 4
+    a, b, c, d = (normed[i * quarter : (i + 1) * quarter] for i in range(4))
+    turned = jnp.concatenate([-b, a, -d, c], axis=0)
+    return normed * cos_table + turned * sin_table
+
+
+def turn_kernel(heads, q_ref, k_ref, v_ref, qg_ref, kg_ref, cos_ref, sin_ref, *out_refs):
+    cos_table, sin_table = cos_ref[...], sin_ref[...]
+    q_gain, k_gain = qg_ref[...], kg_ref[...]
+    for i in range(heads):
+        pair = [
+            turned_head(q_ref[(GROUP * i + g) * HD : (GROUP * i + g + 1) * HD, :], q_gain, cos_table, sin_table)
+            for g in range(GROUP)
+        ]
+        key = turned_head(k_ref[i * HD : (i + 1) * HD, :], k_gain, cos_table, sin_table)
+        value = v_ref[i * HD : (i + 1) * HD, :].astype(jnp.float32)
+        out_ref = out_refs[i]
+        out_ref[0, :, :PAIR] = jnp.concatenate(pair, axis=0).T.astype(jnp.bfloat16)
+        out_ref[0, :, PAIR:] = jnp.concatenate([key, value], axis=0).T.astype(jnp.bfloat16)
+
+
+def turn_and_pack(queries, keys, values, q_gain, k_gain, cos_table, sin_table, sp_count):
+    tok = queries.shape[1]
+    heads = KV // sp_count
+    whole = lambda shape: pl.BlockSpec(shape, lambda d: (0,) * len(shape))
+    return pl.pallas_call(
+        functools.partial(turn_kernel, heads),
+        grid=(sp_count,),
+        in_specs=[
+            pl.BlockSpec((heads * PAIR, tok), lambda d: (d, 0)),
+            pl.BlockSpec((heads * HD, tok), lambda d: (d, 0)),
+            pl.BlockSpec((heads * HD, tok), lambda d: (d, 0)),
+            whole((HD, 1)),
+            whole((HD, 1)),
+            whole((HD, tok)),
+            whole((HD, tok)),
+        ],
+        out_specs=[pl.BlockSpec((1, tok, PAIR + 2 * HD), lambda d: (d, 0, 0))] * heads,
+        out_shape=[jax.ShapeDtypeStruct((sp_count, tok, PAIR + 2 * HD), jnp.bfloat16)] * heads,
+        cost_estimate=pl.CostEstimate(flops=40 * 3072 * tok, bytes_accessed=6 * 4096 * tok, transcendentals=0),
+        name="turn",
+    )(queries, keys, values, q_gain[:, None], k_gain[:, None], cos_table, sin_table)
+
+
+SOFT_ROWS = 16
+
+
+def attend_kernel(seq, rows, q_ref, kv_ref, out_ref, keys_scr, vals_scr, s_scr, w_scr):
+    @pl.when(pl.program_id(0) == 0)
+    def _():
+        kv = kv_ref[...].astype(jnp.float32)
+        lane = lax.broadcasted_iota(jnp.int32, kv.shape, 1)
+        low = lane < HD
+        other = pltpu.roll(kv, HD, 1)
+        keys_scr[0:seq, :] = jnp.where(low, kv, 0.0).astype(jnp.bfloat16)
+        keys_scr[seq : 2 * seq, :] = jnp.where(low, 0.0, other).astype(jnp.bfloat16)
+        vals_scr[0:seq, :] = jnp.where(low, other, 0.0).astype(jnp.bfloat16)
+        vals_scr[seq : 2 * seq, :] = jnp.where(low, 0.0, kv).astype(jnp.bfloat16)
+
+    scale = HD ** (-0.5)
+    s_scr[...] = lax.dot_general(
+        q_ref[...], keys_scr[...], (((1,), (1,)), ((), ())), preferred_element_type=jnp.float32
+    )
+    for g in range(GROUP):
+        for r in range(0, rows, SOFT_ROWS):
+            s = s_scr[r : r + SOFT_ROWS, g * seq : (g + 1) * seq] * scale
+            e = jnp.exp(s - jnp.max(s, axis=-1, keepdims=True))
+            w = e * (1.0 / jnp.sum(e, axis=-1, keepdims=True))
+            w_scr[r : r + SOFT_ROWS, g * seq : (g + 1) * seq] = w.astype(jnp.bfloat16)
+    out_ref[...] = jnp.dot(w_scr[...], vals_scr[...], preferred_element_type=jnp.float32).astype(jnp.bfloat16)
+
+
+def attend(packed):
+    sp_count, tok, _ = packed.shape
+    seq = sp_count * tok
+    flat = packed.reshape(seq, PAIR + 2 * HD)
+    rows = 256 if seq % 256 == 0 else tok
+    return pl.pallas_call(
+        functools.partial(attend_kernel, seq, rows),
+        grid=(seq // rows,),
+        in_specs=[
+            pl.BlockSpec((rows, PAIR), lambda b: (b, 0)),
+            pl.BlockSpec((seq, 2 * HD), lambda b: (0, 1)),
+        ],
+        out_specs=pl.BlockSpec((rows, PAIR), lambda b: (b, 0)),
+        out_shape=jax.ShapeDtypeStruct((seq, PAIR), jnp.bfloat16),
+        scratch_shapes=[
+            pltpu.VMEM((GROUP * seq, 2 * HD), jnp.bfloat16),
+            pltpu.VMEM((GROUP * seq, PAIR), jnp.bfloat16),
+            pltpu.VMEM((rows, GROUP * seq), jnp.float32),
+            pltpu.VMEM((rows, GROUP * seq), jnp.bfloat16),
+        ],
+        cost_estimate=pl.CostEstimate(
+            flops=16 * seq * seq * HD, bytes_accessed=8 * seq * PAIR, transcendentals=GROUP * seq * seq
+        ),
+        name="attend",
+    )(flat, flat).reshape(sp_count, tok, PAIR)
+
+
+def project_kernel(parts, sp_count, att_refs, w_refs, out_ref, bufs, sems):
+    me = lax.axis_index("dp")
+    width = w_refs[0].shape[1]
+    copies = [pltpu.make_async_copy(w_refs[i], bufs.at[i], sems.at[i]) for i in range(parts)]
+    for copy in copies:
+        copy.start()
+    att = jnp.concatenate([att_ref[d] for d in range(sp_count) for att_ref in att_refs], axis=1)
+    for i in range(parts):
+        copies[i].wait()
+        column = pl.multiple_of((me ^ i) * width, width)
+        out_ref[:, pl.ds(column, width)] = jnp.dot(
+            att, bufs[i], preferred_element_type=jnp.float32
+        ).astype(jnp.bfloat16)
+
+
+def project(attended, blocks):
+    parts, heads = len(blocks), len(attended)
+    sp_count, tok, _ = attended[0].shape
+    depth, width = blocks[0].shape
+
+    def body(*refs):
+        project_kernel(parts, sp_count, refs[:heads], refs[heads : heads + parts], *refs[heads + parts :])
+
+    return pl.pallas_call(
+        body,
+        in_specs=[pl.BlockSpec(memory_space=pltpu.VMEM)] * heads + [pl.BlockSpec(memory_space=pl.ANY)] * parts,
+        out_specs=pl.BlockSpec(memory_space=pltpu.VMEM),
+        out_shape=jax.ShapeDtypeStruct((tok, parts * width), jnp.bfloat16),
+        scratch_shapes=[pltpu.VMEM((parts, depth, width), jnp.bfloat16), pltpu.SemaphoreType.DMA((parts,))],
+        cost_estimate=pl.CostEstimate(
+            flops=2 * tok * depth * width * parts, bytes_accessed=2 * depth * width * parts, transcendentals=0
+        ),
+        name="project",
+    )(*attended, *blocks)
+
+
+def column_blocks(w_out):
+    count = lax.axis_size("dp")
+    blocks = {0: w_out}
+    for bit in reversed(range(count.bit_length() - 1)):
+        route = [(i, i ^ (1 << bit)) for i in range(count)]
+        for key in sorted(blocks):
+            blocks[key | (1 << bit)] = lax.ppermute(blocks[key], "dp", route)
+    return [blocks[i] for i in range(count)]
+
+
+def head_form(queries, keys, values, q_gain, k_gain, w_out):
+    sp_count = lax.axis_size("sp")
+    tok = queries.shape[2]
+    blocks = column_blocks(w_out)
+    cos_table, sin_table = rotary_tables(lax.axis_index("sp") * tok, tok)
+    packed = turn_and_pack(queries[0], keys[0], values[0], q_gain, k_gain, cos_table, sin_table, sp_count)
+    attended = []
+    for part in packed:
+        got = lax.all_to_all(part, "sp", split_axis=0, concat_axis=0, tiled=True)
+        attended.append(lax.all_to_all(attend(got), "sp", split_axis=0, concat_axis=0, tiled=True))
+    return project(attended, blocks)[None]
+
+
+def on_device(*args):
+    sp_count, dp_count = lax.axis_size("sp"), lax.axis_size("dp")
+    if KV % sp_count == 0 and dp_count & (dp_count - 1) == 0:
+        return head_form(*args)
+    return plain_form(*args)
+
+
 def solution(mesh):
     placed = (
         P("dp", None, "sp"),

time: 177 us -> 98.2 us (0.55)
  local copies, waits for them, and re-layouts: 43 us -> 7.95 us
  matrix products: 30.5 us -> 0 us
  Pallas kernels: 0 us -> 30.2 us
  other arithmetic: 26 us -> 1.47 us
  blocking collectives: 21.1 us -> 38.5 us
  waiting for transfers between devices: 24 us -> 8.98 us
  between operations: 13.6 us -> 0.05 us
  starting transfers between devices: 18.2 us -> 10.2 us
    pallas_call x0 -> x4, Pallas kernels: none -> 30.2 us  [the longest x2 17.9 us: attend(): pl.pallas_call(functools.partial(attend_kernel, seq, rows), grid=(seq //...]
    convert_element_type x8 -> x0, local copies, waits for them, and re-layouts: 22.7 us -> none  [the longest x6 18.4 us: normalize_turn(): values_f = field.astype(jnp.float32).reshape(head_count, HD, field.shape[1])]
    dot_general x9 -> x0, matrix products: 20.1 us -> none  [the longest x8 14.3 us: one_block(): jnp.einsum('hgqk,hdk->hgdq', weights, value_heads, preferred_element_type...]
    all_to_all x1 -> x2, blocking collectives: 21.1 us -> 38.5 us  [the longest x1 23.4 us: head_form(): got = lax.all_to_all(part, 'sp', split_axis=0, concat_axis=0, tiled=True)]
    all_to_all x3 -> x2, waiting for transfers between devices: 23.3 us -> 5.86 us  [the longest x1 4.49 us: head_form(): got = lax.all_to_all(part, 'sp', split_axis=0, concat_axis=0, tiled=True)]
    mul x2 -> x0, other arithmetic: 12.8 us -> none  [normalize_turn(): values_f * lax.rsqrt(jnp.mean(values_f * values_f, axis=1, keepdims=True)...]
    all_to_all x3 -> x2, starting transfers between devices: 18.2 us -> 7.18 us  [the longest x1 3.64 us: head_form(): lax.all_to_all(attend(got), 'sp', split_axis=0, concat_axis=0, tiled=True)]
    sub x8 -> x0, matrix products: 10.4 us -> none  [one_block(): weights = jnp.exp(scores - row_max)]
  transfers between devices with their start and end apart: 4 -> 5, of which waited for: 2 -> 3; matrix products, arithmetic and copies ran while one was open for 52% -> 10% of each run, Pallas kernels for 0% -> 25%
where the time goes in v1:
time: 98.2 us; the launch traced here: 97.4 us
  blocking collectives  38.5 us (39%)
  Pallas kernels  30.2 us (31%)
  starting transfers between devices  10.2 us (10%)
  waiting for transfers between devices  8.98 us (9%)
  local copies, waits for them, and re-layouts  7.95 us (8%)
  other arithmetic  1.47 us (1%)
    all_to_all x1, blocking collectives, head_form(): got = lax.all_to_all(part, 'sp', split_axis=0, concat_axis=0, tiled=True)  23.4 us
    pallas_call x2, Pallas kernels, attend(): pl.pallas_call(functools.partial(attend_kernel, seq, rows), grid=(seq //...  17.9 us
    all_to_all x1, blocking collectives, head_form(): lax.all_to_all(attend(got), 'sp', split_axis=0, concat_axis=0, tiled=True)  15.2 us
    pallas_call x1, Pallas kernels, turn_and_pack(): pl.pallas_call(functools.partial(turn_kernel, heads), grid=(sp_count,), i...  6.4 us
    pallas_call x1, Pallas kernels, project(): pl.pallas_call(body, in_specs=[pl.BlockSpec(memory_space=pltpu.VMEM)] * h...  5.92 us
    unnamed x11, local copies, waits for them, and re-layouts  5.26 us
    all_to_all x1, waiting for transfers between devices, head_form(): got = lax.all_to_all(part, 'sp', split_axis=0, concat_axis=0, tiled=True)  4.49 us
    all_to_all x1, starting transfers between devices, head_form(): lax.all_to_all(attend(got), 'sp', split_axis=0, concat_axis=0, tiled=True)  3.64 us
  transfers between devices with their start and end apart: 5, of which 3 were waited for; matrix products, arithmetic and copies ran while one was open for 10% of the time, Pallas kernels for 25%

profile of v1, /device:TPU:0, one launch (start us, length us, event | category | flops | bytes accessed | tf_op | source)
XLA Modules:
  0.0 97.4 jit_solution(9356635997126800679)
XLA Ops:
  0.0 0.0 copy-start.2
  0.0 3.0 %collective-permute-start.1 = (bf16[2048,512]{1,0:T(8,128)(2,1)}, bf16[2048,512]{1,0:T(8,128)(2,1)}, u32[]{:S(2)}, u32[]{:S(2)}) collective-permute-start(bf16[2048,512]{1,0:T(8,128)(2,1)} %refs_2_.1), channel_id=1, source_target_pairs={{0,2},{1,3},{2,0},{3,1},{4,6},{5,7},{6,4},{7,5},{8,10},{9,11},{10,... | collective-permute-start | bytes 6291464 | tf_op jit(solution)/shard_map/ppermute | solution.py:283
  3.0 1.3 %copy.10.qg_ref = f32[64,1]{1,0:T(8,128)} copy(f32[64,1]{0,1:T(1,128)} %bitcast.19) | data formatting | bytes 512 | tf_op jit(solution)/shard_map/broadcast_in_dim | solution.py:183
  4.3 1.3 %copy.11.kg_ref = f32[64,1]{1,0:T(8,128)} copy(f32[64,1]{0,1:T(1,128)} %bitcast.20) | data formatting | bytes 512 | tf_op jit(solution)/shard_map/broadcast_in_dim | solution.py:183
  5.7 2.0 %copy.8 = bf16[1,1024,160]{2,1,0:T(8,128)(2,1)} copy(bf16[1,1024,160]{1,2,0:T(8,128)(2,1)} %param.7) | data formatting | bytes 655360 | tf_op args[1]
  7.7 2.0 %copy.9 = bf16[1,1024,160]{2,1,0:T(8,128)(2,1)} copy(bf16[1,1024,160]{1,2,0:T(8,128)(2,1)} %param.8) | data formatting | bytes 655360 | tf_op args[2]
  9.6 0.0 copy-done.2
  9.6 1.3 %copy.7 = bf16[1,2048,160]{2,1,0:T(8,128)(2,1)} copy(bf16[1,2048,160]{1,2,0:T(8,128)(2,1)S(1)} %copy-done.2) | data formatting | bytes 1310720 | tf_op args[0]
  10.9 0.2 multiply_sine_fusion.1
  11.1 0.6 pad_maximum_fusion.1.sin_ref
  11.8 0.6 pad_maximum_fusion.cos_ref
  12.4 0.0 copy-start
  12.4 6.4 %turn.1 = (bf16[8,160,256]{2,1,0:T(8,128)(2,1)}, bf16[8,160,256]{2,1,0:T(8,128)(2,1)}) custom-call(bf16[2048,160]{1,0:T(8,128)(2,1)} %bitcast.10, bf16[1024,160]{1,0:T(8,128)(2,1)} %bitcast.11, bf16[1024,160]{1,0:T(8,128)(2,1)} %bitcast.12, f32[64,1]{1,0:T(8,128)} %copy.10.qg_ref, f32[64,1]{1,0:T(8,128)} %copy.11.kg_ref, f32[64,160]{1,0:T(8,128)} %pad_maximum_fusion.cos_ref, ...), custom_call_target="tpu_custom_call" | custom-call | flops 19660800 | bytes 3932160 | tf_op jit(solution)/shard_map/turn/pallas_call | solution.py:167
  18.8 23.4 %all_to_all.20 = bf16[8,160,256]{2,1,0:T(8,128)(2,1)} all-to-all(bf16[8,160,256]{2,1,0:T(8,128)(2,1)} %get-tuple-element.7), channel_id=1, replica_groups=mesh['sp'=8,'dp'=4] {'sp'}, dimensions={0} | all-to-all | bytes 1310720 | tf_op jit(solution)/shard_map/all_to_all | solution.py:295
  42.2 3.5 %all-to-all-start.2 = ((bf16[8,160,256]{2,1,0:T(8,128)(2,1)}), bf16[8,160,256]{2,1,0:T(8,128)(2,1)S(1)}, u32[]{:S(2)}, u32[]{:S(2)}) async-start(bf16[8,160,256]{2,1,0:T(8,128)(2,1)} %get-tuple-element.8), calls=%async_computation.2 | async-start | bytes 1310720 | tf_op jit(solution)/shard_map/all_to_all | solution.py:295
  45.7 0.0 copy-done
  45.7 0.1 collective-permute-start
  45.8 3.1 %collective-permute-done.1.refs_4_ = bf16[2048,512]{1,0:T(8,128)(2,1)} collective-permute-done((bf16[2048,512]{1,0:T(8,128)(2,1)}, bf16[2048,512]{1,0:T(8,128)(2,1)}, u32[]{:S(2)}, u32[]{:S(2)}) %collective-permute-start.1) | collective-permute-done | bytes 2097184 | tf_op jit(solution)/shard_map/ppermute | solution.py:283
  48.9 0.0 collective-permute-start.2
  48.9 8.9 %attend.2 = bf16[1280,128]{1,0:T(8,128)(2,1)} custom-call(bf16[1280,256]{1,0:T(8,128)(2,1)} %bitcast.15, bf16[1280,256]{1,0:T(8,128)(2,1)} %bitcast.16), custom_call_target="tpu_custom_call" | custom-call | flops 1677721600 | bytes 1310720 | tf_op jit(solution)/shard_map/attend/pallas_call | solution.py:219
  57.9 4.5 %all-to-all-done.2 = bf16[8,160,256]{2,1,0:T(8,128)(2,1)S(1)} async-done(((bf16[8,160,256]{2,1,0:T(8,128)(2,1)}), bf16[8,160,256]{2,1,0:T(8,128)(2,1)S(1)}, u32[]{:S(2)}, u32[]{:S(2)}) %all-to-all-start.2) | async-done | bytes 655392 | tf_op jit(solution)/shard_map/all_to_all | solution.py:295
  62.3 0.0 copy-start.3
  62.3 3.6 %all-to-all-start.1 = ((bf16[8,160,128]{2,1,0:T(8,128)(2,1)}), bf16[8,160,128]{2,1,0:T(8,128)(2,1)S(1)}, u32[]{:S(2)}, u32[]{:S(2)}) async-start(bf16[8,160,128]{2,1,0:T(8,128)(2,1)} %bitcast.17), calls=%async_computation.1 | async-start | bytes 655360 | tf_op jit(solution)/shard_map/all_to_all | solution.py:296
  66.0 0.0 copy-done.3
  66.0 9.0 %attend.3 = bf16[1280,128]{1,0:T(8,128)(2,1)} custom-call(bf16[1280,256]{1,0:T(8,128)(2,1)} %bitcast.13, bf16[1280,256]{1,0:T(8,128)(2,1)} %bitcast.14), custom_call_target="tpu_custom_call" | custom-call | flops 1677721600 | bytes 1310720 | tf_op jit(solution)/shard_map/attend/pallas_call | solution.py:219
  75.0 1.4 %all-to-all-done.1.refs_0_ = bf16[8,160,128]{2,1,0:T(8,128)(2,1)S(1)} async-done(((bf16[8,160,128]{2,1,0:T(8,128)(2,1)}), bf16[8,160,128]{2,1,0:T(8,128)(2,1)S(1)}, u32[]{:S(2)}, u32[]{:S(2)}) %all-to-all-start.1) | async-done | bytes 327712 | tf_op jit(solution)/shard_map/all_to_all | solution.py:296
  76.3 0.0 copy-start.1
  76.3 15.2 %all_to_all.21.refs_1_ = bf16[8,160,128]{2,1,0:T(8,128)(2,1)} all-to-all(bf16[8,160,128]{2,1,0:T(8,128)(2,1)} %bitcast.18), channel_id=1, replica_groups=mesh['sp'=8,'dp'=4] {'sp'}, dimensions={0} | all-to-all | bytes 655360 | tf_op jit(solution)/shard_map/all_to_all | solution.py:296
  91.5 0.0 collective-permute-done.refs_3_
  91.5 0.0 collective-permute-done.2.refs_5_
  91.5 0.0 copy-done.1
  91.5 5.9 %project.1 = bf16[160,2048]{1,0:T(8,128)(2,1)} custom-call(bf16[8,160,128]{2,1,0:T(8,128)(2,1)} %copy-done.1, bf16[8,160,128]{2,1,0:T(8,128)(2,1)} %all_to_all.21.refs_1_, bf16[2048,512]{1,0:T(8,128)(2,1)} %refs_2_.1, bf16[2048,512]{1,0:T(8,128)(2,1)} %collective-permute-done.refs_3_, bf16[2048,512]{1,0:T(8,128)(2,1)} %collective-permute-done.1.refs_4_, ...), custom_call_target="tpu_custom_call" | custom-call | flops 1342177280 | bytes 8388608 | tf_op jit(solution)/shard_map/project/pallas_call | solution.py:264
  (2 shorter events, 0.0 us)
Async XLA Ops:
  0.0 9.6 %copy-start.2 = (bf16[1,2048,160]{1,2,0:T(8,128)(2,1)S(1)}, bf16[1,2048,160]{1,2,0:T(8,128)(2,1)}, u32[]{:S(2)}) copy-start(bf16[1,2048,160]{1,2,0:T(8,128)(2,1)} %param.6) | copy-start | bytes 1966084
  0.0 48.9 %collective-permute-start.1 = (bf16[2048,512]{1,0:T(8,128)(2,1)}, bf16[2048,512]{1,0:T(8,128)(2,1)}, u32[]{:S(2)}, u32[]{:S(2)}) collective-permute-start(bf16[2048,512]{1,0:T(8,128)(2,1)} %refs_2_.1), channel_id=1, source_target_pairs={{0,2},{1,3},{2,0},{3,1},{4,6},{5,7},{6,4},{7,5},{8,10},{9,11},{10,... | collective-permute-start | bytes 6291464 | tf_op jit(solution)/shard_map/ppermute | solution.py:283
  12.4 33.3 %copy-start = (bf16[2048,512]{1,0:T(8,128)(2,1)S(1)}, bf16[2048,512]{1,0:T(8,128)(2,1)}, u32[]{:S(2)}) copy-start(bf16[2048,512]{1,0:T(8,128)(2,1)} %refs_2_.1) | copy-start | bytes 6291460
  42.2 20.2 %all-to-all-start.2 = ((bf16[8,160,256]{2,1,0:T(8,128)(2,1)}), bf16[8,160,256]{2,1,0:T(8,128)(2,1)S(1)}, u32[]{:S(2)}, u32[]{:S(2)}) async-start(bf16[8,160,256]{2,1,0:T(8,128)(2,1)} %get-tuple-element.8), calls=%async_computation.2 | async-start | bytes 1310720 | tf_op jit(solution)/shard_map/all_to_all | solution.py:295
  45.7 45.8 %collective-permute-start = (bf16[2048,512]{1,0:T(8,128)(2,1)S(1)}, bf16[2048,512]{1,0:T(8,128)(2,1)}, u32[]{:S(2)}, u32[]{:S(2)}) collective-permute-start(bf16[2048,512]{1,0:T(8,128)(2,1)S(1)} %copy-done), channel_id=1, source_target_pairs={{0,1},{1,0},{2,3},{3,2},{4,5},{5,4},{6,7},{7,6},{8,9},{9,8},{10,11... | collective-permute-start | bytes 6291464 | tf_op jit(solution)/shard_map/ppermute | solution.py:283
  48.9 42.6 %collective-permute-start.2 = (bf16[2048,512]{1,0:T(8,128)(2,1)}, bf16[2048,512]{1,0:T(8,128)(2,1)}, u32[]{:S(2)}, u32[]{:S(2)}) collective-permute-start(bf16[2048,512]{1,0:T(8,128)(2,1)} %collective-permute-done.1.refs_4_), channel_id=1, source_target_pairs={{0,1},{1,0},{2,3},{3,2},{4,5},{5,4},{6,7},{7,6},{8,9},{9,8},{10,11... | collective-permute-start | bytes 6291464 | tf_op jit(solution)/shard_map/ppermute | solution.py:283
  62.3 3.6 %copy-start.3 = (bf16[8,160,256]{2,1,0:T(8,128)(2,1)}, bf16[8,160,256]{2,1,0:T(8,128)(2,1)S(1)}, u32[]{:S(2)}) copy-start(bf16[8,160,256]{2,1,0:T(8,128)(2,1)S(1)} %all-to-all-done.2) | copy-start | bytes 1966084
  62.3 14.0 %all-to-all-start.1 = ((bf16[8,160,128]{2,1,0:T(8,128)(2,1)}), bf16[8,160,128]{2,1,0:T(8,128)(2,1)S(1)}, u32[]{:S(2)}, u32[]{:S(2)}) async-start(bf16[8,160,128]{2,1,0:T(8,128)(2,1)} %bitcast.17), calls=%async_computation.1 | async-start | bytes 655360 | tf_op jit(solution)/shard_map/all_to_all | solution.py:296
  76.3 15.2 %copy-start.1 = (bf16[8,160,128]{2,1,0:T(8,128)(2,1)}, bf16[8,160,128]{2,1,0:T(8,128)(2,1)S(1)}, u32[]{:S(2)}) copy-start(bf16[8,160,128]{2,1,0:T(8,128)(2,1)S(1)} %all-to-all-done.1.refs_0_) | copy-start | bytes 983044
